TPU v7x, 256 devices: a 4x2x16 block of a 4x16x16 slice. The times are simulated.
256 devices in a mesh: grp: 2 (over y), row: 16 (over z), col: 8 (over x, core).
Axes of the slice: x: 4, y: 2, z: 16, core: 2. Of those that a mesh axis runs over, the one named last changes fastest.
The devices are a block of a 4x16x16 slice.
Arguments:
- tokens: bfloat16 [8192, 2048], P(('grp', 'row')), parts along dimension 0, may hold values from -6 to 6
- w_value: bfloat16 [2048, 2048], P(None, 'col'), may hold values from -0.125 to 0.125
- w_gate_a: bfloat16 [2048, 2048], P(None, 'col'), may hold values from -0.125 to 0.125
- w_gate_b: bfloat16 [2048, 2048], P(None, 'col'), may hold values from -0.125 to 0.125
- short_taps: bfloat16 [3, 3, 2048], replicated, may hold values from -3.5 to 3.5
- pos_weight: float32 [33, 64], replicated, may hold values from -3 to 3
- pos_bias: float32 [64], replicated, may hold values from -3 to 3
- sine_freq: float32 [2, 64], replicated, may hold values from 1.2 to 2
- hid_weight: float32 [64, 64], replicated, may hold values from -1.5 to 1.5
- hid_bias: float32 [64], replicated, may hold values from -3 to 3
- filter_out: float32 [64, 2, 2, 2048], P(None, None, None, 'col'), may hold values from -0.0234375 to 0.0234375
- filter_bias: float32 [2, 2048], replicated, may hold values from -3 to 3
- lag_decay: float32 [2048], replicated, may hold values from 1 to 137, as said below
Outputs:
- mixed: bfloat16 [8192, 2048], P(('grp', 'row'), 'col'), parts along dimension 0
There are 2 independent parts, one for each index of `grp`. A program takes and returns all parts, laid end to end along the dimension named above; an argument that names none is the same for every part. Nothing has to cross between parts.
Inputs may be any that keep to these rules, and one draw needn't show every extreme that they name: `lag_decay`: each channel's envelope decay is positive.
All inputs are finite; a program needn't handle non-finite values.
Results may differ from a plain program's by a relative error of at most 0.0081.
Values may be sent and summed in bfloat16 or wider, within the bound.
A program may use at most 64 MiB of HBM per device.

v0:
```python
import functools
import math

import jax
import jax.numpy as jnp
import numpy as np
from jax import lax
from jax.experimental import pallas as pl
from jax.experimental.pallas import tpu as pltpu
from jax.sharding import PartitionSpec as P

WINDOW_SHIFT = 0.05
MESH = pl.DeviceIdType.MESH
f32 = jnp.float32
bf16 = jnp.bfloat16
SIN_TERMS = 7


def sine_coefficients():
    nodes = 0.5 * np.cos((np.arange(400) + 0.5) * np.pi / 800)
    basis = np.polynomial.chebyshev.Chebyshev.fit(
        nodes * nodes, np.sin(2 * np.pi * nodes) / nodes, SIN_TERMS - 1, domain=[0, 0.25]
    )
    return [float(c) for c in basis.convert(kind=np.polynomial.Polynomial).coef]


def halves(values):
    high = values.astype(jnp.bfloat16)
    low = (values - high.astype(np.float32)).astype(jnp.bfloat16)
    return high, low


def make_constants(count, own, span, feature_total):
    length = count * span
    k1 = np.arange(count)[:, None] + 0.25
    outer = np.exp(2j * np.pi * k1 * np.arange(count)[None, :] / count)
    eye = np.eye(own)
    outer_rows = np.concatenate([np.kron(outer.real, eye), np.kron(outer.imag, eye)], axis=0)
    q = np.arange(span)
    inner = np.exp(2j * np.pi * (q[:, None] * q[None, :] % span) / span)
    turn = np.exp(2j * np.pi * k1 * q[None, :] / length)
    pieces = [*halves(outer_rows.astype(np.float32))]
    for part in (inner.real, inner.imag):
        pieces += [*halves(part.astype(np.float32))]
    forward = np.concatenate(pieces, axis=0)
    backward = np.concatenate([*halves(outer_rows.T.astype(np.float32))], axis=0)
    turns = np.concatenate([turn.real, turn.imag], axis=0).astype(np.float32)
    positions = np.arange(length, dtype=np.float64)
    bands = (feature_total - 1) // 2
    frequencies = np.linspace(1e-4, bands - 1, bands)
    angles = (2.0 * math.pi / length * positions)[None, :] * frequencies[:, None]
    features = np.concatenate(
        [positions[None, :] / max(length - 1, 1), np.cos(angles), -np.sin(angles)], axis=0
    )
    padded = -(-feature_total // 16) * 16
    table = np.zeros((padded, length), np.float32)
    table[:feature_total] = features
    return forward, backward, turns, np.concatenate([*halves(table)], axis=0)


def dot(a, b):
    return jnp.dot(a, b, preferred_element_type=f32)


def dot_nt(a, b):
    return lax.dot_general(a, b, (((1,), (1,)), ((), ())), preferred_element_type=f32)


def split(values):
    high = values.astype(bf16)
    return high, (values - high.astype(f32)).astype(bf16)


def pick(selector, table):
    high = table.astype(bf16)
    rest = table - high.astype(f32)
    middle = rest.astype(bf16)
    low = (rest - middle.astype(f32)).astype(bf16)
    return dot_nt(selector, high) + dot_nt(selector, middle) + dot_nt(selector, low)


def one_hot(rows, columns, first, own):
    row = lax.broadcasted_iota(jnp.int32, (rows, columns), 0)
    column = lax.broadcasted_iota(jnp.int32, (rows, columns), 1)
    return jnp.where(column == first + row % own, 1.0, 0.0).astype(bf16)


def sine_of_turns(turns, coefficients):
    u = turns - jnp.round(turns)
    square = u * u
    total = jnp.full_like(u, coefficients[-1])
    for c in coefficients[-2::-1]:
        total = total * square + c
    return total * u


def kernel(
    count,
    own,
    hid,
    coefficients,
    tokens,
    w_value,
    w_gate_a,
    w_gate_b,
    short_taps,
    pos_weight,
    pos_bias,
    sine_freq,
    hid_weight,
    hid_bias,
    filter_out,
    filter_bias,
    lag_decay,
    features,
    forward,
    backward,
    turns,
    out,
    tok_s,
    wv_s,
    wa_s,
    wb_s,
    taps_s,
    pw_s,
    pb_s,
    sf_s,
    hw_s,
    hb_s,
    fo_s,
    fb_s,
    ld_s,
    feat_s,
    fwd_s,
    bwd_s,
    turn_s,
    pw2_s,
    np_s,
    chan_s,
    send_v,
    send_a,
    send_o,
    recv_v,
    recv_a,
    recv_o,
    edge_send,
    edge_recv,
    gate_s,
    cols_s,
    kin_s,
    spec_s,
    tr_s,
    ti_s,
    local_sem,
    send_sem,
    recv_sem,
):
    me = lax.axis_index("row")
    col = lax.axis_index("col")
    span = tok_s.shape[0]
    share = wv_s.shape[1]
    length = count * span
    barrier = pltpu.get_barrier_semaphore()

    @pl.loop(1, count)
    def _(d):
        pl.semaphore_signal(
            barrier, inc=1, device_id={"row": lax.rem(me + d, count)}, device_id_type=MESH
        )

    start = pl.multiple_of(col * share, share)
    loads = [
        (tokens, tok_s),
        (w_value, wv_s),
        (w_gate_a, wa_s),
        (w_gate_b, wb_s),
        (short_taps.at[:, :, pl.ds(start, share)], taps_s),
        (pos_weight, pw_s),
        (pos_bias, pb_s),
        (sine_freq, sf_s),
        (hid_weight, hw_s),
        (hid_bias, hb_s),
        (filter_out, fo_s),
        (filter_bias.at[:, pl.ds(start, share)], fb_s),
        (lag_decay.at[:, pl.ds(start, share)], ld_s),
        (features, feat_s),
        (forward, fwd_s),
        (backward, bwd_s),
        (turns, turn_s),
    ]
    copies = [pltpu.make_async_copy(s, t, local_sem.at[i]) for i, (s, t) in enumerate(loads)]
    for c in copies:
        c.start()

    def remote(unit, d, source, target):
        to = lax.rem(me + d, count)
        return pltpu.make_async_remote_copy(
            src_ref=source.at[pl.ds(pl.multiple_of(to * own, own), own)],
            dst_ref=target.at[pl.ds(pl.multiple_of(me * own, own), own)],
            send_sem=send_sem.at[unit, d],
            recv_sem=recv_sem.at[unit, d],
            device_id={"row": to},
            device_id_type=MESH,
        )

    def exchange(unit, source, target):
        @pl.loop(0, count - 1)
        def _(i):
            far = lax.div(i + 1, 2)
            d = count // 2 + jnp.where(lax.rem(i, 2) == 1, far, -far)
            remote(unit, d, source, target).start()

        mine = pl.ds(pl.multiple_of(me * own, own), own)
        target[mine, :] = source[mine, :]

    def finish(unit, source, target):
        @pl.loop(1, count)
        def _(d):
            remote(unit, d, source, target).wait_recv()

    def finish_send(unit, source, target):
        @pl.loop(1, count)
        def _(d):
            remote(unit, d, source, target).wait_send()

    copies[0].wait()
    copies[1].wait()
    send_v[...] = dot(tok_s[...], wv_s[...]).T.astype(bf16)
    copies[2].wait()
    send_a[...] = dot(tok_s[...], wa_s[...]).T.astype(bf16)
    pl.semaphore_wait(barrier, count - 1)
    exchange(0, send_v, recv_v)
    exchange(1, send_a, recv_a)

    copies[3].wait()
    gate = dot(tok_s[...], wb_s[...]).astype(bf16).astype(f32)
    gate_s[...] = gate
    edge_send[0] = gate[span - 1 : span, :]
    edge_send[1] = gate[0:1, :]

    def edge(side):
        to = lax.rem(me + (1 if side == 0 else count - 1), count)
        return pltpu.make_async_remote_copy(
            src_ref=edge_send.at[side],
            dst_ref=edge_recv.at[side],
            send_sem=send_sem.at[3, side],
            recv_sem=recv_sem.at[3, side],
            device_id={"row": to},
            device_id_type=MESH,
        )

    edge(0).start()
    edge(1).start()

    for c in copies[4:]:
        c.wait()

    chan_s[...] = jnp.zeros_like(chan_s)
    chan_s[0:3, :] = taps_s[0].astype(f32)
    chan_s[8:11, :] = taps_s[1].astype(f32)
    chan_s[16:18, :] = fb_s[...]
    chan_s[24:25, :] = ld_s[...]
    cols_s[...] = pick(one_hot(count * own, share, me * own, own), chan_s[...])
    hid_eye = one_hot(hid, hid, 0, hid)
    feature_total = pw_s.shape[0]
    padded = feat_s.shape[0] // 2
    pw2_s[...] = jnp.zeros_like(pw2_s)
    pw2_s[0:feature_total, :] = pw_s[...]
    pw2_s[padded : padded + feature_total, :] = pw_s[...]
    np_s[...] = jnp.zeros_like(np_s)
    np_s[0:2, :] = sf_s[...]
    np_s[8:9, :] = pb_s[...]
    np_s[16:17, :] = hb_s[...]
    net = pick(hid_eye, np_s[...])
    scale_a = net[:, 0:1] * (0.5 / math.pi)
    scale_b = net[:, 1:2] * (0.5 / math.pi)
    shift_a = net[:, 8:9] * scale_a
    shift_b = net[:, 16:17] * scale_b
    first_high, first_low = split(pick(hid_eye, pw2_s[...]))
    first_low = first_low[:, :padded]

    def three(table):
        high, low = split(table)
        lane = lax.broadcasted_iota(jnp.int32, table.shape, 1)
        return jnp.where(lane < 2 * hid, high.astype(f32), low.astype(f32)).astype(bf16)

    hw = hw_s[...]
    second = three(pick(hid_eye, jnp.concatenate([hw, hw, hw], axis=0)))
    own_hot = one_hot(own, share, me * own, own)
    weights = []
    for order in range(2):
        for side in range(2):
            w = fo_s[:, order, side, :]
            weights.append(pick(own_hot, jnp.concatenate([w, w, w], axis=0)))
    third = three(jnp.concatenate(weights, axis=0))
    decay = cols_s[0:own, 24:25]

    blocks = 4
    width = length // blocks

    @pl.loop(0, blocks)
    def _(block):
        base = pl.multiple_of(block * width, width)
        feats = feat_s[:, pl.ds(base, width)]
        pre = dot(first_high, feats) + dot(first_low, feats[:padded])
        hidden = sine_of_turns(pre * scale_a + shift_a, coefficients)
        high, low = split(hidden)
        pre = dot(second, jnp.concatenate([high, low, high], axis=0))
        hidden = sine_of_turns(pre * scale_b + shift_b, coefficients)
        high, low = split(hidden)
        raw = dot(third, jnp.concatenate([high, low, high], axis=0))
        position = base + lax.broadcasted_iota(jnp.int32, (own, width), 1)
        scaled = position.astype(f32) * (1.0 / max(length - 1, 1))
        envelope = jnp.exp(-scaled * decay) + WINDOW_SHIFT
        later = jnp.where(position == 0, 0.0, envelope)
        for order in range(2):
            ahead = raw[2 * order * own : (2 * order + 1) * own] * envelope
            behind = raw[(2 * order + 1) * own : (2 * order + 2) * own] * later
            for kind, both in enumerate((ahead + behind, ahead - behind)):
                high, low = split(both)
                for part in range(width // span):
                    row = pl.multiple_of(block * (width // span) * own + part * own, own)
                    lanes = slice(part * span, (part + 1) * span)
                    kin_s[order, kind, 0, pl.ds(row, own), :] = high[:, lanes]
                    kin_s[order, kind, 1, pl.ds(row, own), :] = low[:, lanes]

    rows = count * own
    for part, target in enumerate((tr_s, ti_s)):
        one = turn_s[part * count : (part + 1) * count, :]
        target[...] = jnp.broadcast_to(one[:, None, :], (count, own, span)).reshape(rows, span)

    two = 2 * rows
    outer_high, outer_low = fwd_s.at[0:two], fwd_s.at[two : 2 * two]
    at = 2 * two
    real_high, real_low = fwd_s.at[at : at + span], fwd_s.at[at + span : at + 2 * span]
    at = at + 2 * span
    imag_high, imag_low = fwd_s.at[at : at + span], fwd_s.at[at + span : at + 2 * span]

    def by_real(a):
        return dot(a[0], real_high[...]) + dot(a[1], real_high[...]) + dot(a[0], real_low[...])

    def by_imag(a):
        return dot(a[0], imag_high[...]) + dot(a[1], imag_high[...]) + dot(a[0], imag_low[...])

    def minus(a):
        return (-a[0], -a[1])

    def outer(high, low):
        g = dot(outer_high[...], high) + dot(outer_low[...], high)
        if low is not None:
            g = g + dot(outer_high[...], low)
        real, imag = g[:rows], g[rows:]
        tr, ti = tr_s[...], ti_s[...]
        return split(real * tr - imag * ti), split(real * ti + imag * tr)

    for order in range(2):
        sr, si = outer(kin_s[order, 0, 0], kin_s[order, 0, 1])
        spec_s[order, 0] = (by_real(sr) + by_imag(minus(si))) * (1.0 / length)
        dr, di = outer(kin_s[order, 1, 0], kin_s[order, 1, 1])
        spec_s[order, 1] = (by_imag(dr) + by_real(di)) * (1.0 / length)

    def short(ref, first):
        p = ref[...].astype(f32)
        lane = lax.broadcasted_iota(jnp.int32, (rows, span), 1)
        none = jnp.zeros((own, span), f32)
        back = pltpu.roll(p, 1, 1)
        back = jnp.where(lane == 0, jnp.concatenate([none, back[:-own]], axis=0), back)
        ahead = pltpu.roll(p, span - 1, 1)
        ahead = jnp.where(lane == span - 1, jnp.concatenate([ahead[own:], none], axis=0), ahead)
        tap = [cols_s[:, first + i : first + i + 1] for i in range(3)]
        return (back * tap[0] + p * tap[1] + ahead * tap[2]).astype(bf16)

    def convolve(order, high, low, signal):
        hr, hi = outer(high, low)
        xr = by_real(hr) + by_imag(minus(hi))
        xi = by_imag(hr) + by_real(hi)
        kr, ki = spec_s[order, 0], spec_s[order, 1]
        yr = split(xr * kr - xi * ki)
        yi = split(xr * ki + xi * kr)
        ur = by_real(yr) + by_imag(yi)
        ui = by_real(yi) + by_imag(minus(yr))
        tr, ti = tr_s[...], ti_s[...]
        wr = split(ur * tr + ui * ti)
        wi = split(ui * tr - ur * ti)
        bh = bwd_s[0:rows, :]
        bl = bwd_s[rows : 2 * rows, :]
        y = dot(bh[:, :rows], wr[0]) + dot(bh[:, :rows], wr[1]) + dot(bl[:, :rows], wr[0])
        y = y + dot(bh[:, rows:], wi[0]) + dot(bh[:, rows:], wi[1]) + dot(bl[:, rows:], wi[0])
        return y + signal * cols_s[:, 16 + order : 17 + order]

    finish(0, send_v, recv_v)
    value = short(recv_v, 0)
    first_conv = convolve(0, value, None, value.astype(f32))
    finish(1, send_a, recv_a)
    gated = short(recv_a, 8).astype(f32) * first_conv
    high, low = split(gated)
    send_o[...] = convolve(1, high, low, gated).astype(bf16)
    exchange(2, send_o, recv_o)

    edge(0).wait()
    edge(1).wait()
    gate = gate_s[...]
    row = lax.broadcasted_iota(jnp.int32, (span, share), 0)
    above = jnp.where(me == 0, 0.0, edge_recv[0])
    below = jnp.where(me == count - 1, 0.0, edge_recv[1])
    back = jnp.where(row == 0, above, pltpu.roll(gate, 1, 0))
    ahead = jnp.where(row == span - 1, below, pltpu.roll(gate, span - 1, 0))
    tap = taps_s[2].astype(f32)
    gate = (back * tap[0:1] + gate * tap[1:2] + ahead * tap[2:3]).astype(bf16).astype(f32)
    finish(2, send_o, recv_o)
    out[...] = (gate * recv_o[...].astype(f32).T).astype(bf16)
    finish_send(0, send_v, recv_v)
    finish_send(1, send_a, recv_a)
    finish_send(2, send_o, recv_o)


def per_device(
    tokens,
    w_value,
    w_gate_a,
    w_gate_b,
    short_taps,
    pos_weight,
    pos_bias,
    sine_freq,
    hid_weight,
    hid_bias,
    filter_out,
    filter_bias,
    lag_decay,
):
    count = lax.axis_size("row")
    span, depth = tokens.shape
    share = w_value.shape[1]
    own = share // count
    rows = count * own
    hid = hid_weight.shape[0]
    feature_total = pos_weight.shape[0]
    forward, backward, turns, features = make_constants(count, own, span, feature_total)
    operands = [
        tokens,
        w_value,
        w_gate_a,
        w_gate_b,
        short_taps,
        pos_weight,
        pos_bias[None, :],
        sine_freq,
        hid_weight,
        hid_bias[None, :],
        filter_out,
        filter_bias,
        lag_decay[None, :],
        jnp.asarray(features),
        jnp.asarray(forward),
        jnp.asarray(backward),
        jnp.asarray(turns),
    ]
    cut = {4: (3, 3, share), 11: (2, share), 12: (1, share)}
    landing = [pltpu.VMEM(cut.get(i, x.shape), x.dtype) for i, x in enumerate(operands)]
    square = pltpu.VMEM((rows, span), bf16)
    scratch = [
        *landing,
        pltpu.VMEM((features.shape[0], hid), f32),
        pltpu.VMEM((24, hid), f32),
        pltpu.VMEM((32, share), f32),
        square,
        square,
        square,
        square,
        square,
        square,
        pltpu.VMEM((2, 1, share), f32),
        pltpu.VMEM((2, 1, share), f32),
        pltpu.VMEM((span, share), f32),
        pltpu.VMEM((rows, 32), f32),
        pltpu.VMEM((2, 2, 2, rows, span), bf16),
        pltpu.VMEM((2, 2, rows, span), f32),
        pltpu.VMEM((rows, span), f32),
        pltpu.VMEM((rows, span), f32),
        pltpu.SemaphoreType.DMA((len(operands),)),
        pltpu.SemaphoreType.DMA((4, count)),
        pltpu.SemaphoreType.DMA((4, count)),
    ]
    return pl.pallas_call(
        functools.partial(kernel, count, own, hid, sine_coefficients()),
        out_shape=jax.ShapeDtypeStruct((span, share), bf16),
        in_specs=[pl.BlockSpec(memory_space=pl.ANY)] * len(operands),
        out_specs=pl.BlockSpec(memory_space=pltpu.VMEM),
        scratch_shapes=scratch,
        compiler_params=pltpu.CompilerParams(collective_id=0, has_side_effects=True),
        name="gated_conv",
    )(*operands)


def solution(mesh):
    in_specs = (
        P(("grp", "row"), None),
        P(None, "col"),
        P(None, "col"),
        P(None, "col"),
        P(),
        P(),
        P(),
        P(),
        P(),
        P(),
        P(None, None, None, "col"),
        P(),
        P(),
    )
    out_specs = P(("grp", "row"), "col")
    return jax.shard_map(
        per_device, mesh=mesh, in_specs=in_specs, out_specs=out_specs, check_vma=False
    )
```

profile of v0, /device:TPU:44, one launch (start us, length us, event | category | flops | bytes accessed | tf_op | source)
XLA Modules:
  0.0 54.3 jit_solution(10133379575798806496)
XLA Ops:
  0.0 52.7 %gated_conv.1 = bf16[256,256]{1,0:T(8,128)(2,1)} custom-call(bf16[256,2048]{1,0:T(8,128)(2,1)} %tokens.1, bf16[2048,256]{1,0:T(8,128)(2,1)} %w_value.1, bf16[2048,256]{1,0:T(8,128)(2,1)} %w_gate_a.1, bf16[2048,256]{1,0:T(8,128)(2,1)} %w_gate_b.1, bf16[3,3,2048]{2,1,0:T(4,128)(2,1)} %short_taps.1, f32[33,64]{1,0:T(8,128)} %pos_weight.1, f32[1,64]{1,0:T(1,128)} %bitcast.4, ...), custom_call_target="tpu_custom_call" | custom-call | tf_op jit(solution)/shard_map/gated_conv/pallas_call | solution.py:485
  52.7 1.6 %copy.19 = bf16[256,256]{1,0:T(8,128)(2,1)} copy(bf16[256,256]{1,0:T(8,128)(2,1)} %gated_conv.1) | data formatting | bytes 262144
where the time goes:
time: 54.4 us; the launch traced here: 54.3 us
  Pallas kernels  52.7 us (97%)
  local copies, waits for them, and re-layouts  1.57 us (3%)
    pallas_call x1, Pallas kernels, per_device(): pl.pallas_call(functools.partial(kernel, count, own, hid, sine_coefficien...  52.7 us
    unnamed x1, local copies, waits for them, and re-layouts  1.57 us

commit v1 on v0

--- a/solution.py
+++ b/solution.py
@@ -151,6 +151,8 @@
     spec_s,
     tr_s,
     ti_s,
+    chain_sem,
+    ready_sem,
     local_sem,
     send_sem,
     recv_sem,
@@ -162,11 +164,19 @@
     length = count * span
     barrier = pltpu.get_barrier_semaphore()
 
-    @pl.loop(1, count)
-    def _(d):
-        pl.semaphore_signal(
-            barrier, inc=1, device_id={"row": lax.rem(me + d, count)}, device_id_type=MESH
-        )
+    has_below = me > 0
+    has_above = me < count - 1
+
+    def signal(semaphore, to):
+        pl.semaphore_signal(semaphore, inc=1, device_id={"row": to}, device_id_type=MESH)
+
+    @pl.when(has_below)
+    def _():
+        signal(barrier, me - 1)
+
+    @pl.when(has_above)
+    def _():
+        signal(barrier, me + 1)
 
     start = pl.multiple_of(col * share, share)
     loads = [
@@ -189,11 +199,11 @@
         (turns, turn_s),
     ]
     copies = [pltpu.make_async_copy(s, t, local_sem.at[i]) for i, (s, t) in enumerate(loads)]
-    for c in copies:
+    for c in copies[:3]:
         c.start()
 
-    def remote(unit, d, source, target):
-        to = lax.rem(me + d, count)
+    def remote(unit, to, source, target):
+        d = lax.rem(to - me + count, count)
         return pltpu.make_async_remote_copy(
             src_ref=source.at[pl.ds(pl.multiple_of(to * own, own), own)],
             dst_ref=target.at[pl.ds(pl.multiple_of(me * own, own), own)],
@@ -203,34 +213,55 @@
             device_id_type=MESH,
         )
 
-    def exchange(unit, source, target):
+    def keep(source, target):
+        mine = pl.ds(pl.multiple_of(me * own, own), own)
+        target[mine, :] = source[mine, :]
+
+    def finish(unit, source, target):
+        @pl.loop(1, count)
+        def _(d):
+            remote(unit, lax.rem(me + d, count), source, target).wait_recv()
+
+    def finish_send(unit, source, target):
+        @pl.loop(1, count)
+        def _(d):
+            remote(unit, lax.rem(me + d, count), source, target).wait_send()
+
+    copies[0].wait()
+    copies[1].wait()
+    for c in copies[3:]:
+        c.start()
+    send_v[...] = dot(tok_s[...], wv_s[...]).T.astype(bf16)
+    copies[2].wait()
+    send_a[...] = dot(tok_s[...], wa_s[...]).T.astype(bf16)
+
+    pl.semaphore_wait(barrier, has_below.astype(jnp.int32) + has_above.astype(jnp.int32))
+
+    @pl.when(me > 1)
+    def _():
+        pl.semaphore_wait(chain_sem, 1)
+
+    @pl.when(jnp.logical_and(has_below, has_above))
+    def _():
+        signal(chain_sem, me + 1)
+
+    @pl.loop(0, me)
+    def _(to):
+        signal(ready_sem.at[me], to)
+
+    for unit, source, target in ((0, send_v, recv_v), (1, send_a, recv_a)):
+
         @pl.loop(0, count - 1)
         def _(i):
             far = lax.div(i + 1, 2)
             d = count // 2 + jnp.where(lax.rem(i, 2) == 1, far, -far)
-            remote(unit, d, source, target).start()
-
-        mine = pl.ds(pl.multiple_of(me * own, own), own)
-        target[mine, :] = source[mine, :]
-
-    def finish(unit, source, target):
-        @pl.loop(1, count)
-        def _(d):
-            remote(unit, d, source, target).wait_recv()
-
-    def finish_send(unit, source, target):
-        @pl.loop(1, count)
-        def _(d):
-            remote(unit, d, source, target).wait_send()
-
-    copies[0].wait()
-    copies[1].wait()
-    send_v[...] = dot(tok_s[...], wv_s[...]).T.astype(bf16)
-    copies[2].wait()
-    send_a[...] = dot(tok_s[...], wa_s[...]).T.astype(bf16)
-    pl.semaphore_wait(barrier, count - 1)
-    exchange(0, send_v, recv_v)
-    exchange(1, send_a, recv_a)
+            to = lax.rem(me + d, count)
+
+            @pl.when(to < me)
+            def _():
+                remote(unit, to, source, target).start()
+
+        keep(source, target)
 
     copies[3].wait()
     gate = dot(tok_s[...], wb_s[...]).astype(bf16).astype(f32)
@@ -239,18 +270,22 @@
     edge_send[1] = gate[0:1, :]
 
     def edge(side):
-        to = lax.rem(me + (1 if side == 0 else count - 1), count)
         return pltpu.make_async_remote_copy(
             src_ref=edge_send.at[side],
             dst_ref=edge_recv.at[side],
             send_sem=send_sem.at[3, side],
             recv_sem=recv_sem.at[3, side],
-            device_id={"row": to},
+            device_id={"row": me + (1 if side == 0 else -1)},
             device_id_type=MESH,
         )
 
-    edge(0).start()
-    edge(1).start()
+    @pl.when(has_above)
+    def _():
+        edge(0).start()
+
+    @pl.when(has_below)
+    def _():
+        edge(1).start()
 
     for c in copies[4:]:
         c.wait()
@@ -388,6 +423,12 @@
         y = y + dot(bh[:, rows:], wi[0]) + dot(bh[:, rows:], wi[1]) + dot(bl[:, rows:], wi[0])
         return y + signal * cols_s[:, 16 + order : 17 + order]
 
+    @pl.loop(me + 1, count)
+    def _(to):
+        pl.semaphore_wait(ready_sem.at[to], 1)
+        remote(0, to, send_v, recv_v).start()
+        remote(1, to, send_a, recv_a).start()
+
     finish(0, send_v, recv_v)
     value = short(recv_v, 0)
     first_conv = convolve(0, value, None, value.astype(f32))
@@ -395,10 +436,25 @@
     gated = short(recv_a, 8).astype(f32) * first_conv
     high, low = split(gated)
     send_o[...] = convolve(1, high, low, gated).astype(bf16)
-    exchange(2, send_o, recv_o)
-
-    edge(0).wait()
-    edge(1).wait()
+
+    @pl.loop(0, count)
+    def _(to):
+        @pl.when(to != me)
+        def _():
+            remote(2, to, send_o, recv_o).start()
+
+    keep(send_o, recv_o)
+
+    @pl.when(has_above)
+    def _():
+        edge(0).wait_send()
+        edge(1).wait_recv()
+
+    @pl.when(has_below)
+    def _():
+        edge(1).wait_send()
+        edge(0).wait_recv()
+
     gate = gate_s[...]
     row = lax.broadcasted_iota(jnp.int32, (span, share), 0)
     above = jnp.where(me == 0, 0.0, edge_recv[0])
@@ -478,13 +534,15 @@
         pltpu.VMEM((2, 2, rows, span), f32),
         pltpu.VMEM((rows, span), f32),
         pltpu.VMEM((rows, span), f32),
+        pltpu.SemaphoreType.REGULAR,
+        pltpu.SemaphoreType.REGULAR((count,)),
         pltpu.SemaphoreType.DMA((len(operands),)),
         pltpu.SemaphoreType.DMA((4, count)),
         pltpu.SemaphoreType.DMA((4, count)),
     ]
     return pl.pallas_call(
         functools.partial(kernel, count, own, hid, sine_coefficients()),
-        out_shape=jax.ShapeDtypeStruct((span, share), bf16),
+        out_shape=pltpu.VMEM((span, share), bf16),
         in_specs=[pl.BlockSpec(memory_space=pl.ANY)] * len(operands),
         out_specs=pl.BlockSpec(memory_space=pltpu.VMEM),
         scratch_shapes=scratch,

time: 54.4 us -> 60.2 us (1.11)
  the two profiles are of different devices: /device:TPU:44 before, /device:TPU:160 now
where the time goes in v1:
time: 60.2 us; the launch traced here: 60.1 us
  Pallas kernels  59.4 us (99%)
  local copies, waits for them, and re-layouts  0.66 us (1%)
    pallas_call x1, Pallas kernels, per_device(): pl.pallas_call(functools.partial(kernel, count, own, hid, sine_coefficien...  59.4 us

profile of v1, /device:TPU:160, one launch (start us, length us, event | category | flops | bytes accessed | tf_op | source)
XLA Modules:
  0.0 60.1 jit_solution(7533767715410266793)
XLA Ops:
  0.0 59.4 %gated_conv.1 = bf16[256,256]{1,0:T(8,128)(2,1)S(1)} custom-call(bf16[256,2048]{1,0:T(8,128)(2,1)} %tokens.1, bf16[2048,256]{1,0:T(8,128)(2,1)} %w_value.1, bf16[2048,256]{1,0:T(8,128)(2,1)} %w_gate_a.1, bf16[2048,256]{1,0:T(8,128)(2,1)} %w_gate_b.1, bf16[3,3,2048]{2,1,0:T(4,128)(2,1)} %short_taps.1, f32[33,64]{1,0:T(8,128)} %pos_weight.1, f32[1,64]{1,0:T(1,128)} %bitcast.4, ...), custom_call_target="tpu_custom_call" | custom-call | tf_op jit(solution)/shard_map/gated_conv/pallas_call | solution.py:543
  59.4 0.7 %copy.19 = bf16[256,256]{1,0:T(8,128)(2,1)} copy(bf16[256,256]{1,0:T(8,128)(2,1)S(1)} %gated_conv.1) | data formatting | bytes 262144

commit v2 on v1

--- a/solution.py
+++ b/solution.py
@@ -14,6 +14,7 @@
 f32 = jnp.float32
 bf16 = jnp.bfloat16
 SIN_TERMS = 7
+DATA_PIECES = 2
 
 
 def sine_coefficients():
@@ -137,11 +138,9 @@
     pw2_s,
     np_s,
     chan_s,
-    send_v,
-    send_a,
+    send_va,
+    recv_va,
     send_o,
-    recv_v,
-    recv_a,
     recv_o,
     edge_send,
     edge_recv,
@@ -151,7 +150,6 @@
     spec_s,
     tr_s,
     ti_s,
-    chain_sem,
     ready_sem,
     local_sem,
     send_sem,
@@ -166,17 +164,10 @@
 
     has_below = me > 0
     has_above = me < count - 1
+    rank = lax.rem(me + count - 1, count)
 
     def signal(semaphore, to):
         pl.semaphore_signal(semaphore, inc=1, device_id={"row": to}, device_id_type=MESH)
-
-    @pl.when(has_below)
-    def _():
-        signal(barrier, me - 1)
-
-    @pl.when(has_above)
-    def _():
-        signal(barrier, me + 1)
 
     start = pl.multiple_of(col * share, share)
     loads = [
@@ -202,6 +193,29 @@
     for c in copies[:3]:
         c.start()
 
+    @pl.loop(rank + 1, count)
+    def _(other):
+        signal(barrier, lax.rem(other + 1, count))
+
+    @pl.when(rank > 0)
+    def _():
+        pl.semaphore_wait(barrier, rank)
+
+    @pl.loop(0, rank)
+    def _(other):
+        signal(ready_sem.at[me], lax.rem(other + 1, count))
+
+    def remote_pair(to):
+        d = lax.rem(to - me + count, count)
+        return pltpu.make_async_remote_copy(
+            src_ref=send_va.at[to],
+            dst_ref=recv_va.at[me],
+            send_sem=send_sem.at[0, d],
+            recv_sem=recv_sem.at[0, d],
+            device_id={"row": to},
+            device_id_type=MESH,
+        )
+
     def remote(unit, to, source, target):
         d = lax.rem(to - me + count, count)
         return pltpu.make_async_remote_copy(
@@ -213,55 +227,29 @@
             device_id_type=MESH,
         )
 
-    def keep(source, target):
-        mine = pl.ds(pl.multiple_of(me * own, own), own)
-        target[mine, :] = source[mine, :]
-
-    def finish(unit, source, target):
+    def to_all(body):
         @pl.loop(1, count)
         def _(d):
-            remote(unit, lax.rem(me + d, count), source, target).wait_recv()
-
-    def finish_send(unit, source, target):
-        @pl.loop(1, count)
-        def _(d):
-            remote(unit, lax.rem(me + d, count), source, target).wait_send()
+            body(lax.rem(me + d, count))
 
     copies[0].wait()
     copies[1].wait()
     for c in copies[3:]:
         c.start()
-    send_v[...] = dot(tok_s[...], wv_s[...]).T.astype(bf16)
+    send_va[:, 0] = dot(tok_s[...], wv_s[...]).T.astype(bf16).reshape(count, own, span)
     copies[2].wait()
-    send_a[...] = dot(tok_s[...], wa_s[...]).T.astype(bf16)
-
-    pl.semaphore_wait(barrier, has_below.astype(jnp.int32) + has_above.astype(jnp.int32))
-
-    @pl.when(me > 1)
-    def _():
-        pl.semaphore_wait(chain_sem, 1)
-
-    @pl.when(jnp.logical_and(has_below, has_above))
-    def _():
-        signal(chain_sem, me + 1)
-
-    @pl.loop(0, me)
-    def _(to):
-        signal(ready_sem.at[me], to)
-
-    for unit, source, target in ((0, send_v, recv_v), (1, send_a, recv_a)):
-
-        @pl.loop(0, count - 1)
-        def _(i):
-            far = lax.div(i + 1, 2)
-            d = count // 2 + jnp.where(lax.rem(i, 2) == 1, far, -far)
-            to = lax.rem(me + d, count)
-
-            @pl.when(to < me)
-            def _():
-                remote(unit, to, source, target).start()
-
-        keep(source, target)
+    send_va[:, 1] = dot(tok_s[...], wa_s[...]).T.astype(bf16).reshape(count, own, span)
+
+    @pl.loop(0, count - 1)
+    def _(i):
+        d = lax.div(i, 2) + 1
+        to = lax.rem(me + jnp.where(lax.rem(i, 2) == 0, d, count - d), count)
+
+        @pl.when(lax.rem(to + count - 1, count) < rank)
+        def _():
+            remote_pair(to).start()
+
+    recv_va[me] = send_va[me]
 
     copies[3].wait()
     gate = dot(tok_s[...], wb_s[...]).astype(bf16).astype(f32)
@@ -273,19 +261,11 @@
         return pltpu.make_async_remote_copy(
             src_ref=edge_send.at[side],
             dst_ref=edge_recv.at[side],
-            send_sem=send_sem.at[3, side],
-            recv_sem=recv_sem.at[3, side],
+            send_sem=send_sem.at[2, side],
+            recv_sem=recv_sem.at[2, side],
             device_id={"row": me + (1 if side == 0 else -1)},
             device_id_type=MESH,
         )
-
-    @pl.when(has_above)
-    def _():
-        edge(0).start()
-
-    @pl.when(has_below)
-    def _():
-        edge(1).start()
 
     for c in copies[4:]:
         c.wait()
@@ -371,31 +351,41 @@
     at = at + 2 * span
     imag_high, imag_low = fwd_s.at[at : at + span], fwd_s.at[at + span : at + 2 * span]
 
-    def by_real(a):
-        return dot(a[0], real_high[...]) + dot(a[1], real_high[...]) + dot(a[0], real_low[...])
-
-    def by_imag(a):
-        return dot(a[0], imag_high[...]) + dot(a[1], imag_high[...]) + dot(a[0], imag_low[...])
+    def by(high, low, a, full):
+        total = dot(a[0], high[...])
+        if len(a) > 1:
+            total = total + dot(a[1], high[...])
+        if full:
+            total = total + dot(a[0], low[...])
+        return total
+
+    def by_real(a, full=False):
+        return by(real_high, real_low, a, full)
+
+    def by_imag(a, full=False):
+        return by(imag_high, imag_low, a, full)
 
     def minus(a):
-        return (-a[0], -a[1])
-
-    def outer(high, low):
-        g = dot(outer_high[...], high) + dot(outer_low[...], high)
-        if low is not None:
-            g = g + dot(outer_high[...], low)
+        return tuple(-part for part in a)
+
+    def outer(values, full, pieces):
+        g = dot(outer_high[...], values[0])
+        if len(values) > 1:
+            g = g + dot(outer_high[...], values[1])
+        if full:
+            g = g + dot(outer_low[...], values[0])
         real, imag = g[:rows], g[rows:]
         tr, ti = tr_s[...], ti_s[...]
-        return split(real * tr - imag * ti), split(real * ti + imag * tr)
+        return pieces(real * tr - imag * ti), pieces(real * ti + imag * tr)
 
     for order in range(2):
-        sr, si = outer(kin_s[order, 0, 0], kin_s[order, 0, 1])
-        spec_s[order, 0] = (by_real(sr) + by_imag(minus(si))) * (1.0 / length)
-        dr, di = outer(kin_s[order, 1, 0], kin_s[order, 1, 1])
-        spec_s[order, 1] = (by_imag(dr) + by_real(di)) * (1.0 / length)
-
-    def short(ref, first):
-        p = ref[...].astype(f32)
+        sr, si = outer((kin_s[order, 0, 0], kin_s[order, 0, 1]), True, split)
+        spec_s[order, 0] = (by_real(sr, True) + by_imag(minus(si), True)) * (1.0 / length)
+        dr, di = outer((kin_s[order, 1, 0], kin_s[order, 1, 1]), True, split)
+        spec_s[order, 1] = (by_imag(dr, True) + by_real(di, True)) * (1.0 / length)
+
+    def short(unit, first):
+        p = recv_va[:, unit].reshape(rows, span).astype(f32)
         lane = lax.broadcasted_iota(jnp.int32, (rows, span), 1)
         none = jnp.zeros((own, span), f32)
         back = pltpu.roll(p, 1, 1)
@@ -405,45 +395,54 @@
         tap = [cols_s[:, first + i : first + i + 1] for i in range(3)]
         return (back * tap[0] + p * tap[1] + ahead * tap[2]).astype(bf16)
 
-    def convolve(order, high, low, signal):
-        hr, hi = outer(high, low)
+    def convolve(order, values, signal, pieces):
+        hr, hi = outer(values, False, pieces)
         xr = by_real(hr) + by_imag(minus(hi))
         xi = by_imag(hr) + by_real(hi)
         kr, ki = spec_s[order, 0], spec_s[order, 1]
-        yr = split(xr * kr - xi * ki)
-        yi = split(xr * ki + xi * kr)
+        yr = pieces(xr * kr - xi * ki)
+        yi = pieces(xr * ki + xi * kr)
         ur = by_real(yr) + by_imag(yi)
         ui = by_real(yi) + by_imag(minus(yr))
         tr, ti = tr_s[...], ti_s[...]
-        wr = split(ur * tr + ui * ti)
-        wi = split(ui * tr - ur * ti)
-        bh = bwd_s[0:rows, :]
-        bl = bwd_s[rows : 2 * rows, :]
-        y = dot(bh[:, :rows], wr[0]) + dot(bh[:, :rows], wr[1]) + dot(bl[:, :rows], wr[0])
-        y = y + dot(bh[:, rows:], wi[0]) + dot(bh[:, rows:], wi[1]) + dot(bl[:, rows:], wi[0])
-        return y + signal * cols_s[:, 16 + order : 17 + order]
-
-    @pl.loop(me + 1, count)
-    def _(to):
+        wr = pieces(ur * tr + ui * ti)
+        wi = pieces(ui * tr - ur * ti)
+        y = signal * cols_s[:, 16 + order : 17 + order]
+        for part in wr:
+            y = y + dot(bwd_s[0:rows, 0:rows], part)
+        for part in wi:
+            y = y + dot(bwd_s[0:rows, rows : 2 * rows], part)
+        return y
+
+    @pl.loop(rank + 1, count)
+    def _(other):
+        to = lax.rem(other + 1, count)
         pl.semaphore_wait(ready_sem.at[to], 1)
-        remote(0, to, send_v, recv_v).start()
-        remote(1, to, send_a, recv_a).start()
-
-    finish(0, send_v, recv_v)
-    value = short(recv_v, 0)
-    first_conv = convolve(0, value, None, value.astype(f32))
-    finish(1, send_a, recv_a)
-    gated = short(recv_a, 8).astype(f32) * first_conv
-    high, low = split(gated)
-    send_o[...] = convolve(1, high, low, gated).astype(bf16)
+        remote_pair(to).start()
+
+    @pl.when(has_above)
+    def _():
+        edge(0).start()
+
+    @pl.when(has_below)
+    def _():
+        edge(1).start()
+
+    to_all(lambda to: remote_pair(to).wait_recv())
+    pieces = split if DATA_PIECES == 2 else lambda x: (x.astype(bf16),)
+    value = short(0, 0)
+    first_conv = convolve(0, (value,), value.astype(f32), pieces)
+    gated = short(1, 8).astype(f32) * first_conv
+    send_o[...] = convolve(1, pieces(gated), gated, pieces).astype(bf16)
 
     @pl.loop(0, count)
     def _(to):
         @pl.when(to != me)
         def _():
-            remote(2, to, send_o, recv_o).start()
-
-    keep(send_o, recv_o)
+            remote(1, to, send_o, recv_o).start()
+
+    mine = pl.ds(pl.multiple_of(me * own, own), own)
+    recv_o[mine, :] = send_o[mine, :]
 
     @pl.when(has_above)
     def _():
@@ -463,11 +462,10 @@
     ahead = jnp.where(row == span - 1, below, pltpu.roll(gate, span - 1, 0))
     tap = taps_s[2].astype(f32)
     gate = (back * tap[0:1] + gate * tap[1:2] + ahead * tap[2:3]).astype(bf16).astype(f32)
-    finish(2, send_o, recv_o)
+    to_all(lambda to: remote(1, to, send_o, recv_o).wait_recv())
     out[...] = (gate * recv_o[...].astype(f32).T).astype(bf16)
-    finish_send(0, send_v, recv_v)
-    finish_send(1, send_a, recv_a)
-    finish_send(2, send_o, recv_o)
+    to_all(lambda to: remote_pair(to).wait_send())
+    to_all(lambda to: remote(1, to, send_o, recv_o).wait_send())
 
 
 def per_device(
@@ -520,10 +518,8 @@
         pltpu.VMEM((features.shape[0], hid), f32),
         pltpu.VMEM((24, hid), f32),
         pltpu.VMEM((32, share), f32),
-        square,
-        square,
-        square,
-        square,
+        pltpu.VMEM((count, 2, own, span), bf16),
+        pltpu.VMEM((count, 2, own, span), bf16),
         square,
         square,
         pltpu.VMEM((2, 1, share), f32),
@@ -534,11 +530,10 @@
         pltpu.VMEM((2, 2, rows, span), f32),
         pltpu.VMEM((rows, span), f32),
         pltpu.VMEM((rows, span), f32),
-        pltpu.SemaphoreType.REGULAR,
         pltpu.SemaphoreType.REGULAR((count,)),
         pltpu.SemaphoreType.DMA((len(operands),)),
-        pltpu.SemaphoreType.DMA((4, count)),
-        pltpu.SemaphoreType.DMA((4, count)),
+        pltpu.SemaphoreType.DMA((3, count)),
+        pltpu.SemaphoreType.DMA((3, count)),
     ]
     return pl.pallas_call(
         functools.partial(kernel, count, own, hid, sine_coefficients()),

time: 60.2 us -> 54.1 us (0.90)
  the two profiles are of different devices: /device:TPU:160 before, /device:TPU:44 now
where the time goes in v2:
time: 54.1 us; the launch traced here: 53.8 us
  Pallas kernels  53.1 us (98%)
  local copies, waits for them, and re-layouts  0.66 us (1%)
    pallas_call x1, Pallas kernels, per_device(): pl.pallas_call(functools.partial(kernel, count, own, hid, sine_coefficien...  53.1 us

profile of v2, /device:TPU:44, one launch (start us, length us, event | category | flops | bytes accessed | tf_op | source)
XLA Modules:
  0.0 53.8 jit_solution(10497749201651156077)
XLA Ops:
  0.0 53.1 %gated_conv.1 = bf16[256,256]{1,0:T(8,128)(2,1)S(1)} custom-call(bf16[256,2048]{1,0:T(8,128)(2,1)} %tokens.1, bf16[2048,256]{1,0:T(8,128)(2,1)} %w_value.1, bf16[2048,256]{1,0:T(8,128)(2,1)} %w_gate_a.1, bf16[2048,256]{1,0:T(8,128)(2,1)} %w_gate_b.1, bf16[3,3,2048]{2,1,0:T(4,128)(2,1)} %short_taps.1, f32[33,64]{1,0:T(8,128)} %pos_weight.1, f32[1,64]{1,0:T(1,128)} %bitcast.4, ...), custom_call_target="tpu_custom_call" | custom-call | tf_op jit(solution)/shard_map/gated_conv/pallas_call | solution.py:538
  53.1 0.7 %copy.19 = bf16[256,256]{1,0:T(8,128)(2,1)} copy(bf16[256,256]{1,0:T(8,128)(2,1)S(1)} %gated_conv.1) | data formatting | bytes 262144

commit v3 on v2

--- a/solution.py
+++ b/solution.py
@@ -15,6 +15,7 @@
 bf16 = jnp.bfloat16
 SIN_TERMS = 7
 DATA_PIECES = 2
+LATE = 6
 
 
 def sine_coefficients():
@@ -138,8 +139,10 @@
     pw2_s,
     np_s,
     chan_s,
-    send_va,
-    recv_va,
+    send_v,
+    recv_v,
+    send_a,
+    recv_a,
     send_o,
     recv_o,
     edge_send,
@@ -164,7 +167,15 @@
 
     has_below = me > 0
     has_above = me < count - 1
-    rank = lax.rem(me + count - 1, count)
+    turn_of_first = max(count - 5, 0)
+
+    def rank_of(place):
+        return jnp.where(place == 0, turn_of_first, place - jnp.where(place <= turn_of_first, 1, 0))
+
+    def place_of(turn):
+        return jnp.where(turn == turn_of_first, 0, turn + jnp.where(turn < turn_of_first, 1, 0))
+
+    rank = rank_of(me)
 
     def signal(semaphore, to):
         pl.semaphore_signal(semaphore, inc=1, device_id={"row": to}, device_id_type=MESH)
@@ -195,7 +206,7 @@
 
     @pl.loop(rank + 1, count)
     def _(other):
-        signal(barrier, lax.rem(other + 1, count))
+        signal(barrier, place_of(other))
 
     @pl.when(rank > 0)
     def _():
@@ -203,18 +214,7 @@
 
     @pl.loop(0, rank)
     def _(other):
-        signal(ready_sem.at[me], lax.rem(other + 1, count))
-
-    def remote_pair(to):
-        d = lax.rem(to - me + count, count)
-        return pltpu.make_async_remote_copy(
-            src_ref=send_va.at[to],
-            dst_ref=recv_va.at[me],
-            send_sem=send_sem.at[0, d],
-            recv_sem=recv_sem.at[0, d],
-            device_id={"row": to},
-            device_id_type=MESH,
-        )
+        signal(ready_sem.at[me], place_of(other))
 
     def remote(unit, to, source, target):
         d = lax.rem(to - me + count, count)
@@ -236,114 +236,37 @@
     copies[1].wait()
     for c in copies[3:]:
         c.start()
-    send_va[:, 0] = dot(tok_s[...], wv_s[...]).T.astype(bf16).reshape(count, own, span)
+    mine = pl.ds(pl.multiple_of(me * own, own), own)
+
+    def to_lower(unit, source, target):
+        @pl.loop(0, count - 1)
+        def _(i):
+            d = lax.div(i, 2) + 1
+            to = lax.rem(me + jnp.where(lax.rem(i, 2) == 0, d, count - d), count)
+
+            @pl.when(rank_of(to) < rank)
+            def _():
+                remote(unit, to, source, target).start()
+
+        target[mine, :] = source[mine, :]
+
+    send_v[...] = dot(tok_s[...], wv_s[...]).T.astype(bf16)
+    to_lower(0, send_v, recv_v)
     copies[2].wait()
-    send_va[:, 1] = dot(tok_s[...], wa_s[...]).T.astype(bf16).reshape(count, own, span)
-
-    @pl.loop(0, count - 1)
-    def _(i):
-        d = lax.div(i, 2) + 1
-        to = lax.rem(me + jnp.where(lax.rem(i, 2) == 0, d, count - d), count)
-
-        @pl.when(lax.rem(to + count - 1, count) < rank)
-        def _():
-            remote_pair(to).start()
-
-    recv_va[me] = send_va[me]
-
-    copies[3].wait()
-    gate = dot(tok_s[...], wb_s[...]).astype(bf16).astype(f32)
-    gate_s[...] = gate
-    edge_send[0] = gate[span - 1 : span, :]
-    edge_send[1] = gate[0:1, :]
+    send_a[...] = dot(tok_s[...], wa_s[...]).T.astype(bf16)
+    to_lower(1, send_a, recv_a)
 
     def edge(side):
         return pltpu.make_async_remote_copy(
             src_ref=edge_send.at[side],
             dst_ref=edge_recv.at[side],
-            send_sem=send_sem.at[2, side],
-            recv_sem=recv_sem.at[2, side],
+            send_sem=send_sem.at[3, side],
+            recv_sem=recv_sem.at[3, side],
             device_id={"row": me + (1 if side == 0 else -1)},
             device_id_type=MESH,
         )
 
-    for c in copies[4:]:
-        c.wait()
-
-    chan_s[...] = jnp.zeros_like(chan_s)
-    chan_s[0:3, :] = taps_s[0].astype(f32)
-    chan_s[8:11, :] = taps_s[1].astype(f32)
-    chan_s[16:18, :] = fb_s[...]
-    chan_s[24:25, :] = ld_s[...]
-    cols_s[...] = pick(one_hot(count * own, share, me * own, own), chan_s[...])
-    hid_eye = one_hot(hid, hid, 0, hid)
-    feature_total = pw_s.shape[0]
-    padded = feat_s.shape[0] // 2
-    pw2_s[...] = jnp.zeros_like(pw2_s)
-    pw2_s[0:feature_total, :] = pw_s[...]
-    pw2_s[padded : padded + feature_total, :] = pw_s[...]
-    np_s[...] = jnp.zeros_like(np_s)
-    np_s[0:2, :] = sf_s[...]
-    np_s[8:9, :] = pb_s[...]
-    np_s[16:17, :] = hb_s[...]
-    net = pick(hid_eye, np_s[...])
-    scale_a = net[:, 0:1] * (0.5 / math.pi)
-    scale_b = net[:, 1:2] * (0.5 / math.pi)
-    shift_a = net[:, 8:9] * scale_a
-    shift_b = net[:, 16:17] * scale_b
-    first_high, first_low = split(pick(hid_eye, pw2_s[...]))
-    first_low = first_low[:, :padded]
-
-    def three(table):
-        high, low = split(table)
-        lane = lax.broadcasted_iota(jnp.int32, table.shape, 1)
-        return jnp.where(lane < 2 * hid, high.astype(f32), low.astype(f32)).astype(bf16)
-
-    hw = hw_s[...]
-    second = three(pick(hid_eye, jnp.concatenate([hw, hw, hw], axis=0)))
-    own_hot = one_hot(own, share, me * own, own)
-    weights = []
-    for order in range(2):
-        for side in range(2):
-            w = fo_s[:, order, side, :]
-            weights.append(pick(own_hot, jnp.concatenate([w, w, w], axis=0)))
-    third = three(jnp.concatenate(weights, axis=0))
-    decay = cols_s[0:own, 24:25]
-
-    blocks = 4
-    width = length // blocks
-
-    @pl.loop(0, blocks)
-    def _(block):
-        base = pl.multiple_of(block * width, width)
-        feats = feat_s[:, pl.ds(base, width)]
-        pre = dot(first_high, feats) + dot(first_low, feats[:padded])
-        hidden = sine_of_turns(pre * scale_a + shift_a, coefficients)
-        high, low = split(hidden)
-        pre = dot(second, jnp.concatenate([high, low, high], axis=0))
-        hidden = sine_of_turns(pre * scale_b + shift_b, coefficients)
-        high, low = split(hidden)
-        raw = dot(third, jnp.concatenate([high, low, high], axis=0))
-        position = base + lax.broadcasted_iota(jnp.int32, (own, width), 1)
-        scaled = position.astype(f32) * (1.0 / max(length - 1, 1))
-        envelope = jnp.exp(-scaled * decay) + WINDOW_SHIFT
-        later = jnp.where(position == 0, 0.0, envelope)
-        for order in range(2):
-            ahead = raw[2 * order * own : (2 * order + 1) * own] * envelope
-            behind = raw[(2 * order + 1) * own : (2 * order + 2) * own] * later
-            for kind, both in enumerate((ahead + behind, ahead - behind)):
-                high, low = split(both)
-                for part in range(width // span):
-                    row = pl.multiple_of(block * (width // span) * own + part * own, own)
-                    lanes = slice(part * span, (part + 1) * span)
-                    kin_s[order, kind, 0, pl.ds(row, own), :] = high[:, lanes]
-                    kin_s[order, kind, 1, pl.ds(row, own), :] = low[:, lanes]
-
     rows = count * own
-    for part, target in enumerate((tr_s, ti_s)):
-        one = turn_s[part * count : (part + 1) * count, :]
-        target[...] = jnp.broadcast_to(one[:, None, :], (count, own, span)).reshape(rows, span)
-
     two = 2 * rows
     outer_high, outer_low = fwd_s.at[0:two], fwd_s.at[two : 2 * two]
     at = 2 * two
@@ -378,14 +301,97 @@
         tr, ti = tr_s[...], ti_s[...]
         return pieces(real * tr - imag * ti), pieces(real * ti + imag * tr)
 
-    for order in range(2):
-        sr, si = outer((kin_s[order, 0, 0], kin_s[order, 0, 1]), True, split)
-        spec_s[order, 0] = (by_real(sr, True) + by_imag(minus(si), True)) * (1.0 / length)
-        dr, di = outer((kin_s[order, 1, 0], kin_s[order, 1, 1]), True, split)
-        spec_s[order, 1] = (by_imag(dr, True) + by_real(di, True)) * (1.0 / length)
-
-    def short(unit, first):
-        p = recv_va[:, unit].reshape(rows, span).astype(f32)
+    def prepare():
+        copies[3].wait()
+        gate = dot(tok_s[...], wb_s[...]).astype(bf16).astype(f32)
+        gate_s[...] = gate
+        edge_send[0] = gate[span - 1 : span, :]
+        edge_send[1] = gate[0:1, :]
+
+        for c in copies[4:]:
+            c.wait()
+
+        chan_s[...] = jnp.zeros_like(chan_s)
+        chan_s[0:3, :] = taps_s[0].astype(f32)
+        chan_s[8:11, :] = taps_s[1].astype(f32)
+        chan_s[16:18, :] = fb_s[...]
+        chan_s[24:25, :] = ld_s[...]
+        cols_s[...] = pick(one_hot(count * own, share, me * own, own), chan_s[...])
+        hid_eye = one_hot(hid, hid, 0, hid)
+        feature_total = pw_s.shape[0]
+        padded = feat_s.shape[0] // 2
+        pw2_s[...] = jnp.zeros_like(pw2_s)
+        pw2_s[0:feature_total, :] = pw_s[...]
+        pw2_s[padded : padded + feature_total, :] = pw_s[...]
+        np_s[...] = jnp.zeros_like(np_s)
+        np_s[0:2, :] = sf_s[...]
+        np_s[8:9, :] = pb_s[...]
+        np_s[16:17, :] = hb_s[...]
+        net = pick(hid_eye, np_s[...])
+        scale_a = net[:, 0:1] * (0.5 / math.pi)
+        scale_b = net[:, 1:2] * (0.5 / math.pi)
+        shift_a = net[:, 8:9] * scale_a
+        shift_b = net[:, 16:17] * scale_b
+        first_high, first_low = split(pick(hid_eye, pw2_s[...]))
+        first_low = first_low[:, :padded]
+
+        def three(table):
+            high, low = split(table)
+            lane = lax.broadcasted_iota(jnp.int32, table.shape, 1)
+            return jnp.where(lane < 2 * hid, high.astype(f32), low.astype(f32)).astype(bf16)
+
+        hw = hw_s[...]
+        second = three(pick(hid_eye, jnp.concatenate([hw, hw, hw], axis=0)))
+        own_hot = one_hot(own, share, me * own, own)
+        weights = []
+        for order in range(2):
+            for side in range(2):
+                w = fo_s[:, order, side, :]
+                weights.append(pick(own_hot, jnp.concatenate([w, w, w], axis=0)))
+        third = three(jnp.concatenate(weights, axis=0))
+        decay = cols_s[0:own, 24:25]
+
+        blocks = 4
+        width = length // blocks
+
+        @pl.loop(0, blocks)
+        def _(block):
+            base = pl.multiple_of(block * width, width)
+            feats = feat_s[:, pl.ds(base, width)]
+            pre = dot(first_high, feats) + dot(first_low, feats[:padded])
+            hidden = sine_of_turns(pre * scale_a + shift_a, coefficients)
+            high, low = split(hidden)
+            pre = dot(second, jnp.concatenate([high, low, high], axis=0))
+            hidden = sine_of_turns(pre * scale_b + shift_b, coefficients)
+            high, low = split(hidden)
+            raw = dot(third, jnp.concatenate([high, low, high], axis=0))
+            position = base + lax.broadcasted_iota(jnp.int32, (own, width), 1)
+            scaled = position.astype(f32) * (1.0 / max(length - 1, 1))
+            envelope = jnp.exp(-scaled * decay) + WINDOW_SHIFT
+            later = jnp.where(position == 0, 0.0, envelope)
+            for order in range(2):
+                ahead = raw[2 * order * own : (2 * order + 1) * own] * envelope
+                behind = raw[(2 * order + 1) * own : (2 * order + 2) * own] * later
+                for kind, both in enumerate((ahead + behind, ahead - behind)):
+                    high, low = split(both)
+                    for part in range(width // span):
+                        row = pl.multiple_of(block * (width // span) * own + part * own, own)
+                        lanes = slice(part * span, (part + 1) * span)
+                        kin_s[order, kind, 0, pl.ds(row, own), :] = high[:, lanes]
+                        kin_s[order, kind, 1, pl.ds(row, own), :] = low[:, lanes]
+
+        for part, target in enumerate((tr_s, ti_s)):
+            one = turn_s[part * count : (part + 1) * count, :]
+            target[...] = jnp.broadcast_to(one[:, None, :], (count, own, span)).reshape(rows, span)
+
+        for order in range(2):
+            sr, si = outer((kin_s[order, 0, 0], kin_s[order, 0, 1]), True, split)
+            spec_s[order, 0] = (by_real(sr, True) + by_imag(minus(si), True)) * (1.0 / length)
+            dr, di = outer((kin_s[order, 1, 0], kin_s[order, 1, 1]), True, split)
+            spec_s[order, 1] = (by_imag(dr, True) + by_real(di, True)) * (1.0 / length)
+
+    def short(ref, first):
+        p = ref[...].astype(f32)
         lane = lax.broadcasted_iota(jnp.int32, (rows, span), 1)
         none = jnp.zeros((own, span), f32)
         back = pltpu.roll(p, 1, 1)
@@ -414,11 +420,20 @@
             y = y + dot(bwd_s[0:rows, rows : 2 * rows], part)
         return y
 
-    @pl.loop(rank + 1, count)
-    def _(other):
-        to = lax.rem(other + 1, count)
-        pl.semaphore_wait(ready_sem.at[to], 1)
-        remote_pair(to).start()
+    late = (rank >= count - LATE).astype(jnp.int32)
+
+    @pl.loop(0, 2)
+    def _(step):
+        pl.when(step == late)(prepare)
+
+        @pl.when(step != late)
+        def _():
+            @pl.loop(rank + 1, count)
+            def _(other):
+                to = place_of(other)
+                pl.semaphore_wait(ready_sem.at[to], 1)
+                remote(0, to, send_v, recv_v).start()
+                remote(1, to, send_a, recv_a).start()
 
     @pl.when(has_above)
     def _():
@@ -428,20 +443,20 @@
     def _():
         edge(1).start()
 
-    to_all(lambda to: remote_pair(to).wait_recv())
+    to_all(lambda to: remote(0, to, send_v, recv_v).wait_recv())
     pieces = split if DATA_PIECES == 2 else lambda x: (x.astype(bf16),)
-    value = short(0, 0)
+    value = short(recv_v, 0)
     first_conv = convolve(0, (value,), value.astype(f32), pieces)
-    gated = short(1, 8).astype(f32) * first_conv
+    to_all(lambda to: remote(1, to, send_a, recv_a).wait_recv())
+    gated = short(recv_a, 8).astype(f32) * first_conv
     send_o[...] = convolve(1, pieces(gated), gated, pieces).astype(bf16)
 
     @pl.loop(0, count)
     def _(to):
         @pl.when(to != me)
         def _():
-            remote(1, to, send_o, recv_o).start()
-
-    mine = pl.ds(pl.multiple_of(me * own, own), own)
+            remote(2, to, send_o, recv_o).start()
+
     recv_o[mine, :] = send_o[mine, :]
 
     @pl.when(has_above)
@@ -462,10 +477,11 @@
     ahead = jnp.where(row == span - 1, below, pltpu.roll(gate, span - 1, 0))
     tap = taps_s[2].astype(f32)
     gate = (back * tap[0:1] + gate * tap[1:2] + ahead * tap[2:3]).astype(bf16).astype(f32)
-    to_all(lambda to: remote(1, to, send_o, recv_o).wait_recv())
+    to_all(lambda to: remote(0, to, send_v, recv_v).wait_send())
+    to_all(lambda to: remote(1, to, send_a, recv_a).wait_send())
+    to_all(lambda to: remote(2, to, send_o, recv_o).wait_send())
+    to_all(lambda to: remote(2, to, send_o, recv_o).wait_recv())
     out[...] = (gate * recv_o[...].astype(f32).T).astype(bf16)
-    to_all(lambda to: remote_pair(to).wait_send())
-    to_all(lambda to: remote(1, to, send_o, recv_o).wait_send())
 
 
 def per_device(
@@ -518,8 +534,10 @@
         pltpu.VMEM((features.shape[0], hid), f32),
         pltpu.VMEM((24, hid), f32),
         pltpu.VMEM((32, share), f32),
-        pltpu.VMEM((count, 2, own, span), bf16),
-        pltpu.VMEM((count, 2, own, span), bf16),
+        square,
+        square,
+        square,
+        square,
         square,
         square,
         pltpu.VMEM((2, 1, share), f32),
@@ -532,8 +550,8 @@
         pltpu.VMEM((rows, span), f32),
         pltpu.SemaphoreType.REGULAR((count,)),
         pltpu.SemaphoreType.DMA((len(operands),)),
-        pltpu.SemaphoreType.DMA((3, count)),
-        pltpu.SemaphoreType.DMA((3, count)),
+        pltpu.SemaphoreType.DMA((4, count)),
+        pltpu.SemaphoreType.DMA((4, count)),
     ]
     return pl.pallas_call(
         functools.partial(kernel, count, own, hid, sine_coefficients()),

time: 54.1 us -> 52.8 us (0.976)
  Pallas kernels: 53.1 us -> 52 us
    pallas_call x1, Pallas kernels: 53.1 us -> 52 us  [per_device(): pl.pallas_call(functools.partial(kernel, count, own, hid, sine_coefficien...]
where the time goes in v3:
time: 52.8 us; the launch traced here: 52.7 us
  Pallas kernels  52 us (98%)
  local copies, waits for them, and re-layouts  0.66 us (1%)
    pallas_call x1, Pallas kernels, per_device(): pl.pallas_call(functools.partial(kernel, count, own, hid, sine_coefficien...  52 us

profile of v3, /device:TPU:44, one launch (start us, length us, event | category | flops | bytes accessed | tf_op | source)
XLA Modules:
  0.0 52.7 jit_solution(8517848416905132705)
XLA Ops:
  0.0 52.0 %gated_conv.1 = bf16[256,256]{1,0:T(8,128)(2,1)S(1)} custom-call(bf16[256,2048]{1,0:T(8,128)(2,1)} %tokens.1, bf16[2048,256]{1,0:T(8,128)(2,1)} %w_value.1, bf16[2048,256]{1,0:T(8,128)(2,1)} %w_gate_a.1, bf16[2048,256]{1,0:T(8,128)(2,1)} %w_gate_b.1, bf16[3,3,2048]{2,1,0:T(4,128)(2,1)} %short_taps.1, f32[33,64]{1,0:T(8,128)} %pos_weight.1, f32[1,64]{1,0:T(1,128)} %bitcast.4, ...), custom_call_target="tpu_custom_call" | custom-call | tf_op jit(solution)/shard_map/gated_conv/pallas_call | solution.py:556
  52.0 0.7 %copy.19 = bf16[256,256]{1,0:T(8,128)(2,1)} copy(bf16[256,256]{1,0:T(8,128)(2,1)S(1)} %gated_conv.1) | data formatting | bytes 262144

commit v4 on v3

--- a/solution.py
+++ b/solution.py
@@ -15,7 +15,6 @@
 bf16 = jnp.bfloat16
 SIN_TERMS = 7
 DATA_PIECES = 2
-LATE = 6
 
 
 def sine_coefficients():
@@ -301,7 +300,18 @@
         tr, ti = tr_s[...], ti_s[...]
         return pieces(real * tr - imag * ti), pieces(real * ti + imag * tr)
 
+    def serve(turn):
+        to = place_of(turn)
+        pl.semaphore_wait(ready_sem.at[to], 1)
+        remote(0, to, send_v, recv_v).start()
+        remote(1, to, send_a, recv_a).start()
+
+    def serve_next(steps):
+        pl.when(rank + steps < count)(lambda: serve(rank + steps))
+
     def prepare():
+        serve_next(1)
+        serve_next(2)
         copies[3].wait()
         gate = dot(tok_s[...], wb_s[...]).astype(bf16).astype(f32)
         gate_s[...] = gate
@@ -350,6 +360,8 @@
                 weights.append(pick(own_hot, jnp.concatenate([w, w, w], axis=0)))
         third = three(jnp.concatenate(weights, axis=0))
         decay = cols_s[0:own, 24:25]
+
+        serve_next(3)
 
         blocks = 4
         width = length // blocks
@@ -380,6 +392,10 @@
                         kin_s[order, kind, 0, pl.ds(row, own), :] = high[:, lanes]
                         kin_s[order, kind, 1, pl.ds(row, own), :] = low[:, lanes]
 
+            @pl.when(lax.rem(block, 2) == 1)
+            def _():
+                serve_next(4 + lax.div(block, 2))
+
         for part, target in enumerate((tr_s, ti_s)):
             one = turn_s[part * count : (part + 1) * count, :]
             target[...] = jnp.broadcast_to(one[:, None, :], (count, own, span)).reshape(rows, span)
@@ -389,6 +405,8 @@
             spec_s[order, 0] = (by_real(sr, True) + by_imag(minus(si), True)) * (1.0 / length)
             dr, di = outer((kin_s[order, 1, 0], kin_s[order, 1, 1]), True, split)
             spec_s[order, 1] = (by_imag(dr, True) + by_real(di, True)) * (1.0 / length)
+            if order == 0:
+                serve_next(6)
 
     def short(ref, first):
         p = ref[...].astype(f32)
@@ -420,20 +438,11 @@
             y = y + dot(bwd_s[0:rows, rows : 2 * rows], part)
         return y
 
-    late = (rank >= count - LATE).astype(jnp.int32)
-
-    @pl.loop(0, 2)
-    def _(step):
-        pl.when(step == late)(prepare)
-
-        @pl.when(step != late)
-        def _():
-            @pl.loop(rank + 1, count)
-            def _(other):
-                to = place_of(other)
-                pl.semaphore_wait(ready_sem.at[to], 1)
-                remote(0, to, send_v, recv_v).start()
-                remote(1, to, send_a, recv_a).start()
+    prepare()
+
+    @pl.loop(rank + 7, count)
+    def _(turn):
+        serve(turn)
 
     @pl.when(has_above)
     def _():

time: 52.8 us -> 51.4 us (0.973)
  Pallas kernels: 52 us -> 50.6 us
    pallas_call x1, Pallas kernels: 52 us -> 50.6 us  [per_device(): pl.pallas_call(functools.partial(kernel, count, own, hid, sine_coefficien...]
where the time goes in v4:
time: 51.4 us; the launch traced here: 51.3 us
  Pallas kernels  50.6 us (98%)
  local copies, waits for them, and re-layouts  0.66 us (1%)
    pallas_call x1, Pallas kernels, per_device(): pl.pallas_call(functools.partial(kernel, count, own, hid, sine_coefficien...  50.6 us

profile of v4, /device:TPU:44, one launch (start us, length us, event | category | flops | bytes accessed | tf_op | source)
XLA Modules:
  0.0 51.3 jit_solution(7817143927910190113)
XLA Ops:
  0.0 50.6 %gated_conv.1 = bf16[256,256]{1,0:T(8,128)(2,1)S(1)} custom-call(bf16[256,2048]{1,0:T(8,128)(2,1)} %tokens.1, bf16[2048,256]{1,0:T(8,128)(2,1)} %w_value.1, bf16[2048,256]{1,0:T(8,128)(2,1)} %w_gate_a.1, bf16[2048,256]{1,0:T(8,128)(2,1)} %w_gate_b.1, bf16[3,3,2048]{2,1,0:T(4,128)(2,1)} %short_taps.1, f32[33,64]{1,0:T(8,128)} %pos_weight.1, f32[1,64]{1,0:T(1,128)} %bitcast.4, ...), custom_call_target="tpu_custom_call" | custom-call | tf_op jit(solution)/shard_map/gated_conv/pallas_call | solution.py:565
  50.6 0.7 %copy.19 = bf16[256,256]{1,0:T(8,128)(2,1)} copy(bf16[256,256]{1,0:T(8,128)(2,1)S(1)} %gated_conv.1) | data formatting | bytes 262144

commit v5 on v4

--- a/solution.py
+++ b/solution.py
@@ -240,8 +240,9 @@
     def to_lower(unit, source, target):
         @pl.loop(0, count - 1)
         def _(i):
-            d = lax.div(i, 2) + 1
-            to = lax.rem(me + jnp.where(lax.rem(i, 2) == 0, d, count - d), count)
+            step = lax.div(i + 1, 2)
+            d = count // 2 + jnp.where(lax.rem(i, 2) == 1, step, -step)
+            to = lax.rem(me + d, count)
 
             @pl.when(rank_of(to) < rank)
             def _():
@@ -300,14 +301,15 @@
         tr, ti = tr_s[...], ti_s[...]
         return pieces(real * tr - imag * ti), pieces(real * ti + imag * tr)
 
-    def serve(turn):
-        to = place_of(turn)
+    def serve(to):
         pl.semaphore_wait(ready_sem.at[to], 1)
         remote(0, to, send_v, recv_v).start()
         remote(1, to, send_a, recv_a).start()
 
+    serve_base = jnp.where(me == 0, turn_of_first, me)
+
     def serve_next(steps):
-        pl.when(rank + steps < count)(lambda: serve(rank + steps))
+        pl.when(serve_base + steps < count)(lambda: serve(serve_base + steps))
 
     def prepare():
         serve_next(1)
@@ -440,9 +442,13 @@
 
     prepare()
 
-    @pl.loop(rank + 7, count)
-    def _(turn):
-        serve(turn)
+    @pl.loop(serve_base + 7, count)
+    def _(to):
+        serve(to)
+
+    @pl.when(rank < turn_of_first)
+    def _():
+        serve(0)
 
     @pl.when(has_above)
     def _():

time: 51.4 us -> 50.4 us (0.981)
  Pallas kernels: 50.6 us -> 49.6 us
    pallas_call x1, Pallas kernels: 50.6 us -> 49.6 us  [per_device(): pl.pallas_call(functools.partial(kernel, count, own, hid, sine_coefficien...]
where the time goes in v5:
time: 50.4 us; the launch traced here: 50.2 us
  Pallas kernels  49.6 us (98%)
  local copies, waits for them, and re-layouts  0.66 us (1%)
    pallas_call x1, Pallas kernels, per_device(): pl.pallas_call(functools.partial(kernel, count, own, hid, sine_coefficien...  49.6 us

profile of v5, /device:TPU:44, one launch (start us, length us, event | category | flops | bytes accessed | tf_op | source)
XLA Modules:
  0.0 50.2 jit_solution(9191073369833148636)
XLA Ops:
  0.0 49.6 %gated_conv.1 = bf16[256,256]{1,0:T(8,128)(2,1)S(1)} custom-call(bf16[256,2048]{1,0:T(8,128)(2,1)} %tokens.1, bf16[2048,256]{1,0:T(8,128)(2,1)} %w_value.1, bf16[2048,256]{1,0:T(8,128)(2,1)} %w_gate_a.1, bf16[2048,256]{1,0:T(8,128)(2,1)} %w_gate_b.1, bf16[3,3,2048]{2,1,0:T(4,128)(2,1)} %short_taps.1, f32[33,64]{1,0:T(8,128)} %pos_weight.1, f32[1,64]{1,0:T(1,128)} %bitcast.4, ...), custom_call_target="tpu_custom_call" | custom-call | tf_op jit(solution)/shard_map/gated_conv/pallas_call | solution.py:571
  49.6 0.7 %copy.19 = bf16[256,256]{1,0:T(8,128)(2,1)} copy(bf16[256,256]{1,0:T(8,128)(2,1)S(1)} %gated_conv.1) | data formatting | bytes 262144

commit v6 on v5

--- a/solution.py
+++ b/solution.py
@@ -14,7 +14,6 @@
 f32 = jnp.float32
 bf16 = jnp.bfloat16
 SIN_TERMS = 7
-DATA_PIECES = 2
 
 
 def sine_coefficients():
@@ -421,18 +420,21 @@
         tap = [cols_s[:, first + i : first + i + 1] for i in range(3)]
         return (back * tap[0] + p * tap[1] + ahead * tap[2]).astype(bf16)
 
-    def convolve(order, values, signal, pieces):
-        hr, hi = outer(values, False, pieces)
+    def one(values):
+        return (values.astype(bf16),)
+
+    def convolve(order, values, signal):
+        hr, hi = outer(values, False, one)
         xr = by_real(hr) + by_imag(minus(hi))
         xi = by_imag(hr) + by_real(hi)
         kr, ki = spec_s[order, 0], spec_s[order, 1]
-        yr = pieces(xr * kr - xi * ki)
-        yi = pieces(xr * ki + xi * kr)
+        yr = one(xr * kr - xi * ki)
+        yi = one(xr * ki + xi * kr)
         ur = by_real(yr) + by_imag(yi)
         ui = by_real(yi) + by_imag(minus(yr))
         tr, ti = tr_s[...], ti_s[...]
-        wr = pieces(ur * tr + ui * ti)
-        wi = pieces(ui * tr - ur * ti)
+        wr = split(ur * tr + ui * ti)
+        wi = split(ui * tr - ur * ti)
         y = signal * cols_s[:, 16 + order : 17 + order]
         for part in wr:
             y = y + dot(bwd_s[0:rows, 0:rows], part)
@@ -459,12 +461,11 @@
         edge(1).start()
 
     to_all(lambda to: remote(0, to, send_v, recv_v).wait_recv())
-    pieces = split if DATA_PIECES == 2 else lambda x: (x.astype(bf16),)
     value = short(recv_v, 0)
-    first_conv = convolve(0, (value,), value.astype(f32), pieces)
+    first_conv = convolve(0, (value,), value.astype(f32))
     to_all(lambda to: remote(1, to, send_a, recv_a).wait_recv())
     gated = short(recv_a, 8).astype(f32) * first_conv
-    send_o[...] = convolve(1, pieces(gated), gated, pieces).astype(bf16)
+    send_o[...] = convolve(1, split(gated), gated).astype(bf16)
 
     @pl.loop(0, count)
     def _(to):

time: 50.4 us -> 50 us (level)
  no operation moved by 1% of the time
where the time goes in v6:
time: 50 us; the launch traced here: 49.9 us
  Pallas kernels  49.2 us (98%)
  local copies, waits for them, and re-layouts  0.66 us (1%)
    pallas_call x1, Pallas kernels, per_device(): pl.pallas_call(functools.partial(kernel, count, own, hid, sine_coefficien...  49.2 us

profile of v6, /device:TPU:44, one launch (start us, length us, event | category | flops | bytes accessed | tf_op | source)
XLA Modules:
  0.0 49.9 jit_solution(10527526089628610184)
XLA Ops:
  0.0 49.2 %gated_conv.1 = bf16[256,256]{1,0:T(8,128)(2,1)S(1)} custom-call(bf16[256,2048]{1,0:T(8,128)(2,1)} %tokens.1, bf16[2048,256]{1,0:T(8,128)(2,1)} %w_value.1, bf16[2048,256]{1,0:T(8,128)(2,1)} %w_gate_a.1, bf16[2048,256]{1,0:T(8,128)(2,1)} %w_gate_b.1, bf16[3,3,2048]{2,1,0:T(4,128)(2,1)} %short_taps.1, f32[33,64]{1,0:T(8,128)} %pos_weight.1, f32[1,64]{1,0:T(1,128)} %bitcast.4, ...), custom_call_target="tpu_custom_call" | custom-call | tf_op jit(solution)/shard_map/gated_conv/pallas_call | solution.py:572
  49.2 0.7 %copy.19 = bf16[256,256]{1,0:T(8,128)(2,1)} copy(bf16[256,256]{1,0:T(8,128)(2,1)S(1)} %gated_conv.1) | data formatting | bytes 262144

commit v7 on v6

--- a/solution.py
+++ b/solution.py
@@ -165,7 +165,7 @@
 
     has_below = me > 0
     has_above = me < count - 1
-    turn_of_first = max(count - 5, 0)
+    turn_of_first = max(count - 7, 0)
 
     def rank_of(place):
         return jnp.where(place == 0, turn_of_first, place - jnp.where(place <= turn_of_first, 1, 0))
@@ -309,6 +309,15 @@
 
     def serve_next(steps):
         pl.when(serve_base + steps < count)(lambda: serve(serve_base + steps))
+
+    def serve_rest(steps):
+        @pl.loop(serve_base + steps, count)
+        def _(to):
+            serve(to)
+
+        @pl.when(rank < turn_of_first)
+        def _():
+            serve(0)
 
     def prepare():
         serve_next(1)
@@ -407,7 +416,7 @@
             dr, di = outer((kin_s[order, 1, 0], kin_s[order, 1, 1]), True, split)
             spec_s[order, 1] = (by_imag(dr, True) + by_real(di, True)) * (1.0 / length)
             if order == 0:
-                serve_next(6)
+                serve_rest(6)
 
     def short(ref, first):
         p = ref[...].astype(f32)
@@ -443,14 +452,6 @@
         return y
 
     prepare()
-
-    @pl.loop(serve_base + 7, count)
-    def _(to):
-        serve(to)
-
-    @pl.when(rank < turn_of_first)
-    def _():
-        serve(0)
 
     @pl.when(has_above)
     def _():

time: 50 us -> 48.6 us (0.972)
  Pallas kernels: 49.2 us -> 47.7 us
    pallas_call x1, Pallas kernels: 49.2 us -> 47.7 us  [per_device(): pl.pallas_call(functools.partial(kernel, count, own, hid, sine_coefficien...]
where the time goes in v7:
time: 48.6 us; the launch traced here: 48.4 us
  Pallas kernels  47.7 us (98%)
  local copies, waits for them, and re-layouts  0.66 us (1%)
    pallas_call x1, Pallas kernels, per_device(): pl.pallas_call(functools.partial(kernel, count, own, hid, sine_coefficien...  47.7 us

profile of v7, /device:TPU:44, one launch (start us, length us, event | category | flops | bytes accessed | tf_op | source)
XLA Modules:
  0.0 48.4 jit_solution(11956535204592283448)
XLA Ops:
  0.0 47.7 %gated_conv.1 = bf16[256,256]{1,0:T(8,128)(2,1)S(1)} custom-call(bf16[256,2048]{1,0:T(8,128)(2,1)} %tokens.1, bf16[2048,256]{1,0:T(8,128)(2,1)} %w_value.1, bf16[2048,256]{1,0:T(8,128)(2,1)} %w_gate_a.1, bf16[2048,256]{1,0:T(8,128)(2,1)} %w_gate_b.1, bf16[3,3,2048]{2,1,0:T(4,128)(2,1)} %short_taps.1, f32[33,64]{1,0:T(8,128)} %pos_weight.1, f32[1,64]{1,0:T(1,128)} %bitcast.4, ...), custom_call_target="tpu_custom_call" | custom-call | tf_op jit(solution)/shard_map/gated_conv/pallas_call | solution.py:573
  47.7 0.7 %copy.19 = bf16[256,256]{1,0:T(8,128)(2,1)} copy(bf16[256,256]{1,0:T(8,128)(2,1)S(1)} %gated_conv.1) | data formatting | bytes 262144

commit v8 on v7

--- a/solution.py
+++ b/solution.py
@@ -165,7 +165,7 @@
 
     has_below = me > 0
     has_above = me < count - 1
-    turn_of_first = max(count - 7, 0)
+    turn_of_first = max(count - 8, 0)
 
     def rank_of(place):
         return jnp.where(place == 0, turn_of_first, place - jnp.where(place <= turn_of_first, 1, 0))

time: 48.6 us -> 49.6 us (1.021)
  the two profiles are of different devices: /device:TPU:44 before, /device:TPU:160 now
where the time goes in v8:
time: 49.6 us; the launch traced here: 49.5 us
  Pallas kernels  48.8 us (98%)
  local copies, waits for them, and re-layouts  0.66 us (1%)
    pallas_call x1, Pallas kernels, per_device(): pl.pallas_call(functools.partial(kernel, count, own, hid, sine_coefficien...  48.8 us

profile of v8, /device:TPU:160, one launch (start us, length us, event | category | flops | bytes accessed | tf_op | source)
XLA Modules:
  0.0 49.5 jit_solution(16978434555161218679)
XLA Ops:
  0.0 48.8 %gated_conv.1 = bf16[256,256]{1,0:T(8,128)(2,1)S(1)} custom-call(bf16[256,2048]{1,0:T(8,128)(2,1)} %tokens.1, bf16[2048,256]{1,0:T(8,128)(2,1)} %w_value.1, bf16[2048,256]{1,0:T(8,128)(2,1)} %w_gate_a.1, bf16[2048,256]{1,0:T(8,128)(2,1)} %w_gate_b.1, bf16[3,3,2048]{2,1,0:T(4,128)(2,1)} %short_taps.1, f32[33,64]{1,0:T(8,128)} %pos_weight.1, f32[1,64]{1,0:T(1,128)} %bitcast.4, ...), custom_call_target="tpu_custom_call" | custom-call | tf_op jit(solution)/shard_map/gated_conv/pallas_call | solution.py:573
  48.8 0.7 %copy.19 = bf16[256,256]{1,0:T(8,128)(2,1)} copy(bf16[256,256]{1,0:T(8,128)(2,1)S(1)} %gated_conv.1) | data formatting | bytes 262144
